TPU v7x, 128 devices: a whole 4x4x4 slice. The times are simulated.
128 devices in a mesh: ep: 16 (over z, x), tp: 8 (over y, core).
Axes of the slice: x: 4, y: 4, z: 4, core: 2. Of those that a mesh axis runs over, the one named last changes fastest.
Arguments:
- hidden_in: bfloat16 [256, 2048], P(None, 'ep'), may hold values from -24 to 24
- attn_gain: float32 [2048], replicated, may hold values from 0.1 to 1.9
- forget_weight: bfloat16 [2048, 16], replicated, may hold values from -0.125 to 0.125
- forget_bias: float32 [16], replicated, may hold values from -1 to 2
- query_weight: bfloat16 [2048, 2048], P('ep', 'tp'), may hold values from -0.125 to 0.125
- key_weight: bfloat16 [2048, 1024], P('ep', 'tp'), may hold values from -0.125 to 0.125
- value_weight: bfloat16 [2048, 1024], P('ep', 'tp'), may hold values from -0.125 to 0.125
- query_gain: float32 [128], replicated, may hold values from 0.1 to 1.9
- key_gain: float32 [128], replicated, may hold values from 0.1 to 1.9
- cache_keys: bfloat16 [256, 8, 1024, 128], P('ep', 'tp'), may hold values from -160 to 160
- cache_values: bfloat16 [256, 8, 1024, 128], P('ep', 'tp'), may hold values from -6 to 6
- cache_gates: float32 [256, 16, 1024], P('ep', 'tp'), may hold values from -256 to 0, as said below
- lengths: int32 [256], P('ep'), may hold values from 128 to 1024, as said below
- output_weight: bfloat16 [2048, 2048], P('tp', 'ep'), may hold values from -0.125 to 0.125
- ffn_gain: float32 [2048], replicated, may hold values from 0.1 to 1.9
- route_group: int32 [256], replicated, may hold values from 0 to 7, as said below
- route_expert: int32 [256, 2], replicated, may hold values from 0 to 3, as said below
- route_weight: float32 [256, 2], replicated, may hold values from 0.1 to 0.6
- expert_gate: bfloat16 [32, 2048, 1024], P('ep', None, 'tp'), may hold values from -0.125 to 0.125
- expert_up: bfloat16 [32, 2048, 1024], P('ep', None, 'tp'), may hold values from -0.125 to 0.125
- expert_down: bfloat16 [32, 1024, 2048], P('ep', 'tp'), may hold values from -0.1875 to 0.1875
- mix_vector: bfloat16 [2048], replicated, may hold values from -0.125 to 0.125
- dense_gate: bfloat16 [2048, 4096], P('ep', 'tp'), may hold values from -0.125 to 0.125
- dense_up: bfloat16 [2048, 4096], P('ep', 'tp'), may hold values from -0.125 to 0.125
- dense_down: bfloat16 [4096, 2048], P('tp', 'ep'), may hold values from -0.09375 to 0.09375
Outputs:
- mixed: bfloat16 [256, 2048], P(None, 'ep')
- fresh_keys: bfloat16 [256, 1024], P('ep', 'tp')
- fresh_values: bfloat16 [256, 1024], P('ep', 'tp')
Inputs may be any that keep to these rules, and one draw needn't show every extreme that they name: `cache_gates`: never rising along positions. `lengths`: some device holds a sequence of length 1024 in every draw. `route_group`: no expert is chosen by more than 24 tokens of the batch, and some expert by exactly 24. `route_expert`: a token's 2 experts differ; the loads of the experts of one group differ by at most two.
All inputs are finite; a program needn't handle non-finite values.
Results may differ from a plain program's by a relative error of at most 0.008.
Values may be sent and summed in bfloat16 or wider, within the bound.
A program may use at most 64 MiB of HBM per device.

v0:
```python
import jax
import jax.numpy as jnp
from jax import lax
from jax.sharding import Mesh
from jax.sharding import PartitionSpec as P

D = 2048
HEAD_DIM = 128
GROUP_EXPERTS = 4
TOPK = 2
CAPACITY = 24
EP = ("ep_0", "ep_1")


EPS = 1e-06


def from_everyone(shard, axis):
    copies = jnp.broadcast_to(shard, (lax.axis_size(axis), *shard.shape))
    return lax.all_to_all(copies, axis, split_axis=0, concat_axis=0, tiled=True)


def of_everyone(shard, axis):
    everything = from_everyone(shard, axis)
    return jnp.sum(everything, axis=0)


def together(arrays, axis):
    ends = [0]
    for a in arrays:
        ends.append(ends[-1] + a.size)
    total = of_everyone(jnp.concatenate([a.ravel() for a in arrays]), axis)
    return tuple((total[b:e].reshape(a.shape) for a, b, e in zip(arrays, ends, ends[1:])))


def split_up(shard, dim, devices):
    lengths = shard.shape
    blocks = shard.reshape(*lengths[:dim], devices, lengths[dim] // devices, *lengths[dim + 1 :])
    return jnp.moveaxis(blocks, dim, 0)


def summed_on_arrival(shard, axis, dim):
    blocks = split_up(shard, dim, lax.axis_size(axis))
    arrived = lax.all_to_all(blocks, axis, split_axis=0, concat_axis=0, tiled=True)
    return arrived.astype(jnp.float32).sum(axis=0)


def in_order(blocks, dim):
    lengths = list(blocks.shape[1:])
    lengths[dim] *= blocks.shape[0]
    return jnp.moveaxis(blocks, 0, dim).reshape(lengths)


def gathered_copies(shard, axis, dim):
    return in_order(from_everyone(shard, axis), dim)


def taken_together(shard, axis):
    return from_everyone(shard, axis).astype(jnp.float32).sum(axis=0)


def by_axis(shard, axes):
    for axis in axes:
        shard = lax.psum(shard, axis)
    return shard


def head_norm(projected, gain_vec):
    return (
        projected
        * lax.rsqrt(jnp.mean(projected * projected, axis=-1, keepdims=True) + EPS)
        * gain_vec
    )


def slot_targets(route_group, route_expert, expert_count):
    chosen = (route_group[:, None] * GROUP_EXPERTS + route_expert).reshape(-1)
    onehot = (chosen[:, None] == jnp.arange(expert_count, dtype=jnp.int32)[None, :]).astype(
        jnp.int32
    )
    before = jnp.cumsum(onehot, axis=0) - onehot
    return chosen * CAPACITY + jnp.sum(before * onehot, axis=1)


def on_device(
    hidden_in,
    attn_gain,
    forget_weight,
    forget_bias,
    query_weight,
    key_weight,
    value_weight,
    query_gain,
    key_gain,
    cache_keys,
    cache_values,
    cache_gates,
    lengths,
    output_weight,
    ffn_gain,
    route_group,
    route_expert,
    route_weight,
    expert_gate,
    expert_up,
    expert_down,
    mix_vector,
    dense_gate,
    dense_up,
    dense_down,
):
    seq_count, width_block = hidden_in.shape
    own_count = cache_keys.shape[0]
    ep_index = lax.axis_index(EP)
    tp_index = lax.axis_index("tp")
    ep_count = lax.axis_size(EP)
    col_start = ep_index * width_block
    row_start = ep_index * own_count
    stream = hidden_in.astype(jnp.float32)
    normed_in = (stream * lax.dynamic_slice_in_dim(attn_gain, col_start, width_block)).astype(
        jnp.bfloat16
    )
    forget_rows = lax.dynamic_slice_in_dim(forget_weight, col_start, width_block, 0)
    squares, forget_dot = together(
        (
            jnp.sum(stream * stream, axis=1),
            jnp.dot(normed_in, forget_rows, preferred_element_type=jnp.float32),
        ),
        EP,
    )
    inv_rms = lax.rsqrt(squares / D + EPS)
    query_cols = query_weight.shape[1]
    key_cols = key_weight.shape[1]
    selected = normed_in
    head_sums = summed_on_arrival(
        jnp.concatenate(
            [
                jnp.dot(selected, query_weight, preferred_element_type=jnp.float32),
                jnp.dot(selected, key_weight, preferred_element_type=jnp.float32),
                jnp.dot(selected, value_weight, preferred_element_type=jnp.float32),
            ],
            axis=1,
        ).astype(jnp.bfloat16),
        EP,
        0,
    )
    heads_here = query_cols // HEAD_DIM
    kv_here = key_cols // HEAD_DIM
    group_size = heads_here // kv_here
    own_scale = lax.dynamic_slice_in_dim(inv_rms, row_start, own_count)
    query_rows = head_norm(
        head_sums[:, :query_cols].reshape(own_count, heads_here, HEAD_DIM), query_gain
    ).astype(jnp.bfloat16)
    fresh_key = head_norm(
        head_sums[:, query_cols : query_cols + key_cols].reshape(own_count, kv_here, HEAD_DIM),
        key_gain,
    ).astype(jnp.bfloat16)
    fresh_value = (head_sums[:, query_cols + key_cols :] * own_scale[:, None]).astype(jnp.bfloat16)
    gate_logit = lax.dynamic_slice(
        forget_dot, (row_start, tp_index * heads_here), (own_count, heads_here)
    )
    bias_here = lax.dynamic_slice_in_dim(forget_bias, tp_index * heads_here, heads_here)
    log_forget = jax.nn.log_sigmoid(gate_logit * own_scale[:, None] + bias_here)
    latest = jnp.take_along_axis(cache_gates, (lengths - 1)[:, None, None], axis=2)[:, :, 0]
    now_gate = (latest + log_forget).reshape(own_count, kv_here, group_size)
    grouped = query_rows.reshape(own_count, kv_here, group_size, HEAD_DIM)
    factor = HEAD_DIM ** (-0.5)
    scores = (
        jnp.einsum("skgd,skcd->skgc", grouped, cache_keys, preferred_element_type=jnp.float32)
        * factor
    )
    scores = scores + now_gate[..., None] - cache_gates.reshape(own_count, kv_here, group_size, -1)
    in_cache = (
        jnp.arange(cache_keys.shape[2], dtype=jnp.int32)[None, None, None, :]
        < lengths[:, None, None, None]
    )
    scores = jnp.where(in_cache, scores, -jnp.inf)
    self_score = (
        jnp.einsum("skgd,skd->skg", grouped, fresh_key, preferred_element_type=jnp.float32) * factor
    )
    ceiling = jnp.maximum(jnp.max(scores, axis=-1), self_score)
    weights = jnp.exp(scores - ceiling[..., None])
    self_weight = jnp.exp(self_score - ceiling)
    denominator = jnp.sum(weights, axis=-1) + self_weight
    mixed_heads = jnp.einsum(
        "skgc,skcd->skgd",
        weights.astype(jnp.bfloat16),
        cache_values,
        preferred_element_type=jnp.float32,
    )
    mixed_heads = mixed_heads + self_weight[..., None] * fresh_value.reshape(
        own_count, kv_here, 1, HEAD_DIM
    ).astype(jnp.float32)
    heads_out = (
        (mixed_heads / denominator[..., None]).reshape(own_count, query_cols).astype(jnp.bfloat16)
    )
    attn_part = jnp.dot(
        gathered_copies(heads_out, EP, 0), output_weight, preferred_element_type=jnp.float32
    )
    attn_out = taken_together(attn_part.astype(jnp.bfloat16), "tp").astype(jnp.float32)
    middle = (stream + attn_out).astype(jnp.bfloat16).astype(jnp.float32)
    normed_mid = (middle * lax.dynamic_slice_in_dim(ffn_gain, col_start, width_block)).astype(
        jnp.bfloat16
    )
    mix_part = jnp.dot(
        normed_mid,
        lax.dynamic_slice_in_dim(mix_vector, col_start, width_block),
        preferred_element_type=jnp.float32,
    )
    squares_mid, mix_dot = (by_axis(jnp.sum(middle * middle, axis=1), EP), by_axis(mix_part, EP))
    mid_scale = lax.rsqrt(squares_mid / D + EPS)
    mix_share = jax.nn.sigmoid(mid_scale * mix_dot)
    local_experts = expert_gate.shape[0]
    expert_count = local_experts * ep_count
    targets = slot_targets(route_group, route_expert, expert_count)
    slot_total = expert_count * CAPACITY
    slot_ids = jnp.arange(slot_total, dtype=jnp.int32)
    placed = jnp.any(
        targets.reshape(seq_count, TOPK)[None, :, :] == slot_ids[:, None, None], axis=2
    )
    outgoing = jnp.dot(placed.astype(jnp.bfloat16), normed_mid, preferred_element_type=jnp.float32)
    outgoing = outgoing.astype(jnp.bfloat16).reshape(ep_count, local_experts, CAPACITY, width_block)
    arrived = lax.all_to_all(outgoing, EP, split_axis=0, concat_axis=3, tiled=True).reshape(
        local_experts, CAPACITY, -1
    )
    my_slots = lax.dynamic_slice_in_dim(
        placed, ep_index * local_experts * CAPACITY, local_experts * CAPACITY, 0
    )
    slot_scale = jnp.sum(jnp.where(my_slots, mid_scale[None, :], 0.0), axis=1).reshape(
        local_experts, CAPACITY, 1
    )
    gate_pre = (
        jnp.einsum("ecd,edf->ecf", arrived, expert_gate, preferred_element_type=jnp.float32)
        * slot_scale
    )
    up_pre = (
        jnp.einsum("ecd,edf->ecf", arrived, expert_up, preferred_element_type=jnp.float32)
        * slot_scale
    )
    expert_hidden = (jax.nn.silu(gate_pre) * up_pre).astype(jnp.bfloat16)
    expert_part = jnp.einsum(
        "ecf,efd->ecd", expert_hidden, expert_down, preferred_element_type=jnp.float32
    )
    returned = (
        lax.all_to_all(
            expert_part[None].astype(jnp.bfloat16), EP, split_axis=3, concat_axis=0, tiled=True
        )
        .astype(jnp.float32)
        .reshape(slot_total, width_block)
    )
    picked = jnp.take(returned, targets, axis=0).reshape(seq_count, TOPK, width_block)
    routed = jnp.sum(picked * route_weight[:, :, None], axis=1)
    hidden_width = dense_gate.shape[1]
    selected = normed_mid
    both_sums = summed_on_arrival(
        jnp.concatenate(
            [
                jnp.dot(selected, dense_gate, preferred_element_type=jnp.float32),
                jnp.dot(selected, dense_up, preferred_element_type=jnp.float32),
            ],
            axis=1,
        ).astype(jnp.bfloat16),
        EP,
        0,
    )
    gate_sum = both_sums[:, :hidden_width]
    up_sum = both_sums[:, hidden_width:]
    own_mid = lax.dynamic_slice_in_dim(mid_scale, row_start, own_count)
    dense_hidden = (jax.nn.silu(gate_sum * own_mid[:, None]) * (up_sum * own_mid[:, None])).astype(
        jnp.bfloat16
    )
    dense_part = jnp.dot(
        gathered_copies(dense_hidden, EP, 0), dense_down, preferred_element_type=jnp.float32
    )
    ffn_total = taken_together(
        (routed + mix_share[:, None] * dense_part).astype(jnp.bfloat16), "tp"
    ).astype(jnp.float32)
    mixed = (middle + ffn_total).astype(jnp.bfloat16)
    return (mixed, fresh_key.reshape(own_count, key_cols), fresh_value)


def solution(mesh):
    torus = Mesh(mesh.devices.reshape(4, 4, mesh.shape["tp"]), ("ep_0", "ep_1", "tp"))
    placed = (
        P(None, EP),
        P(),
        P(),
        P(),
        P(EP, "tp"),
        P(EP, "tp"),
        P(EP, "tp"),
        P(),
        P(),
        P(EP, "tp", None, None),
        P(EP, "tp", None, None),
        P(EP, "tp", None),
        P(EP),
        P("tp", EP),
        P(),
        P(),
        P(),
        P(),
        P(EP, None, "tp"),
        P(EP, None, "tp"),
        P(EP, "tp", None),
        P(),
        P(EP, "tp"),
        P(EP, "tp"),
        P("tp", EP),
    )
    return jax.shard_map(
        on_device,
        mesh=torus,
        in_specs=placed,
        out_specs=(P(None, EP), P(EP, "tp"), P(EP, "tp")),
        check_vma=False,
    )
```

profile of v0, /device:TPU:1, one launch (start us, length us, event | category | flops | bytes accessed | tf_op | source)
XLA Modules:
  0.0 158.2 jit_solution(674005669819975293)
XLA Ops:
  0.7 0.8 dynamic_slice.27
  1.5 1.0 convolution_convert_fusion.4
  2.5 1.0 convolution_convert_fusion.6
  3.5 1.0 convolution_convert_fusion.5
  4.5 0.7 pad_maximum_fusion.1
  5.3 8.4 %all-to-all-start = ((bf16[16,16,512]{2,1,0:T(8,128)(2,1)}), bf16[16,16,512]{2,1,0:T(8,128)(2,1)S(1)}, u32[]{:S(2)}, u32[]{:S(2)}) async-start(bf16[16,16,512]{2,1,0:T(8,128)(2,1)} %pad_maximum_fusion.1), calls=%async_computation | async-start | bytes 524288 | tf_op jit(solution)/shard_map/all_to_all | solution.py:44
  13.7 1.0 fusion.32
  14.7 0.7 fusion.76
  15.3 0.7 compare_and_fusion.1
  16.0 1.0 fusion.50
  17.1 0.7 broadcast_multiply_fusion.1
  17.8 0.7 broadcast_multiply_fusion
  18.6 0.1 eq.39
  18.9 5.6 %copy.68 = f32[16,2,1024]{1,2,0:T(8,128)} copy(f32[16,2,1024]{2,1,0:T(2,128)} %param.36) | data formatting | bytes 262144 | tf_op args[11]
  24.5 1.1 reduce-window.6
  25.7 1.3 gather_fusion.1
  27.1 0.8 broadcast_in_dim.84
  27.9 6.7 %all-to-all-start.1 = ((f32[16,1,4352]{2,1,0:T(1,128)}), f32[16,1,4352]{2,1,0:T(1,128)S(1)}, u32[]{:S(2)}, u32[]{:S(2)}) async-start(f32[16,1,4352]{2,1,0:T(1,128)} %broadcast_in_dim.84), calls=%async_computation.1 | async-start | bytes 557056 | tf_op jit(solution)/shard_map/all_to_all | solution.py:20
  35.0 7.2 %all-to-all-done.1 = f32[16,1,4352]{2,1,0:T(1,128)S(1)} async-done(((f32[16,1,4352]{2,1,0:T(1,128)}), f32[16,1,4352]{2,1,0:T(1,128)S(1)}, u32[]{:S(2)}, u32[]{:S(2)}) %all-to-all-start.1) | async-done | bytes 278560 | tf_op jit(solution)/shard_map/all_to_all | solution.py:20
  42.2 0.2 reduce_sum.124
  42.6 0.7 fusion.80
  43.6 3.7 %fusion.83 = (f32[16,2]{1,0:T(8,128)S(1)}, f32[16,2,1024]{2,1,0:T(2,128)S(1)}) fusion(f32[16,2,1024]{2,1,0:T(2,128)S(1)} %copy-done.3, f32[16,2]{1,0:T(8,128)S(1)} %fusion.65, bf16[16,2,128]{2,1,0:T(2,128)(2,1)S(1)} %multiply_convert_fusion, bf16[16,1,1024,128]{3,2,1,0:T(8,128)(2,1)} %param.34, pred[16,1024]{1,0:T(8,128)(4,1)S(1)} %iota_compare_fusion.3), kind=kOutput, calls=%fused_computation.120 | convolution fusion | flops 8552416 | bytes 4481280 | tf_op jit(solution)/shard_map/skgd,skcd->skgc/dot_general | solution.py:169
  47.3 0.2 fusion.37
  47.6 0.7 fusion.25
  48.3 0.7 broadcast_in_dim.86
  49.0 3.5 %all-to-all-start.2 = ((bf16[16,16,256]{2,1,0:T(8,128)(2,1)}), bf16[16,16,256]{2,1,0:T(8,128)(2,1)S(1)}, u32[]{:S(2)}, u32[]{:S(2)}) async-start(bf16[16,16,256]{2,1,0:T(8,128)(2,1)} %broadcast_in_dim.86), calls=%async_computation.2 | async-start | bytes 262144 | tf_op jit(solution)/shard_map/all_to_all | solution.py:20
  52.5 0.2 slice_reduce_fusion
  52.7 0.1 reshape.286
  53.0 0.1 reduce_sum.129
  53.3 6.1 %all-to-all-done.2 = bf16[16,16,256]{2,1,0:T(8,128)(2,1)S(1)} async-done(((bf16[16,16,256]{2,1,0:T(8,128)(2,1)}), bf16[16,16,256]{2,1,0:T(8,128)(2,1)S(1)}, u32[]{:S(2)}, u32[]{:S(2)}) %all-to-all-start.2) | async-done | bytes 131104 | tf_op jit(solution)/shard_map/all_to_all | solution.py:20
  59.3 0.2 convolution_convert_fusion.7
  59.5 0.9 broadcast_in_dim.87
  60.3 8.3 %all-to-all-start.3 = ((bf16[8,256,128]{2,1,0:T(8,128)(2,1)}), bf16[8,256,128]{2,1,0:T(8,128)(2,1)S(1)}, u32[]{:S(2)}, u32[]{:S(2)}) async-start(bf16[8,256,128]{2,1,0:T(8,128)(2,1)} %broadcast_in_dim.87), calls=%async_computation.3 | async-start | bytes 1048576 | tf_op jit(solution)/shard_map/all_to_all | solution.py:20
  68.6 0.8 dynamic_slice.32
  69.5 0.1 mul.267
  69.7 0.3 fusion.5
  70.0 8.0 %all-to-all-done.3 = bf16[8,256,128]{2,1,0:T(8,128)(2,1)S(1)} async-done(((bf16[8,256,128]{2,1,0:T(8,128)(2,1)}), bf16[8,256,128]{2,1,0:T(8,128)(2,1)S(1)}, u32[]{:S(2)}, u32[]{:S(2)}) %all-to-all-start.3) | async-done | bytes 524320 | tf_op jit(solution)/shard_map/all_to_all | solution.py:20
  78.2 0.2 convolution_convert_fusion.2
  78.4 0.2 convolution_convert_fusion.1
  78.6 0.9 fusion.47
  79.5 1.0 convolution_convert_fusion.3
  80.4 3.5 %all-to-all-start.4 = ((bf16[16,2,24,128]{3,2,1,0:T(8,128)(2,1)}), bf16[16,2,24,128]{3,2,1,0:T(8,128)(2,1)S(1)}, u32[]{:S(2)}, u32[]{:S(2)}) async-start(bf16[16,2,24,128]{3,2,1,0:T(8,128)(2,1)} %bitcast.13), calls=%async_computation.4 | async-start | bytes 393216 | tf_op jit(solution)/shard_map/all_to_all | solution.py:223
  84.0 0.9 pad_maximum_fusion
  84.8 8.8 %all-reduce.1 = (f32[256]{0:T(256)S(1)}, f32[256]{0:T(256)S(1)}) all-reduce(f32[256]{0:T(256)S(1)} %get-tuple-element.11, f32[256]{0:T(256)S(1)} %bitcast.119), channel_id=1, replica_groups=mesh['ep_0'=4,'ep_1'=4,'tp'=8] {'ep_0'}, use_global_device_ids=true, to_apply=%region_13.14 | all-reduce | flops 512 | bytes 4096 | tf_op jit(solution)/shard_map/psum | solution.py:64
  93.6 8.1 %all-reduce = (f32[256]{0:T(256)S(1)}, f32[256]{0:T(256)S(1)}) all-reduce(f32[256]{0:T(256)S(1)} %get-tuple-element.5, f32[256]{0:T(256)S(1)} %get-tuple-element.6), channel_id=1, replica_groups=mesh['ep_0'=4,'ep_1'=4,'tp'=8] {'ep_1'}, use_global_device_ids=true, to_apply=%region_14.15 | all-reduce | flops 512 | bytes 4096 | tf_op jit(solution)/shard_map/psum | solution.py:64
  101.7 3.6 %all-to-all-start.6 = ((bf16[16,16,1024]{2,1,0:T(8,128)(2,1)}), bf16[16,16,1024]{2,1,0:T(8,128)(2,1)S(1)}, u32[]{:S(2)}, u32[]{:S(2)}) async-start(bf16[16,16,1024]{2,1,0:T(8,128)(2,1)} %pad_maximum_fusion), calls=%async_computation.6 | async-start | bytes 1048576 | tf_op jit(solution)/shard_map/all_to_all | solution.py:44
  105.8 0.3 convolution_multiply_fusion.2
  106.1 1.7 %fusion.4 = bf16[1,2,24,2048]{3,2,1,0:T(8,128)(2,1)S(1)} fusion(bf16[2,128,2048]{2,1,0:T(8,128)(2,1)S(1)} %copy-done, bf16[2,24,2048]{2,1,0:T(8,128)(2,1)S(1)} %reshape.289, bf16[2,2048,128]{2,1,0:T(8,128)(2,1)} %param.44, f32[2,24,128]{2,1,0:T(8,128)S(1)} %convolution_multiply_fusion.2, f32[2,24]{1,0:T(2,128)S(1)} %mul.261), kind=kOutput, calls=%fused_computation.7 | convolution fusion | flops 50472960 | bytes 2515136 | tf_op jit(solution)/shard_map/ecf,efd->ecd/dot_general | solution.py:241
  107.7 0.7 copy.77
  108.5 2.0 %reshape.315 = bf16[16,2,3072]{2,1,0:T(2,128)(2,1)} reshape(bf16[2048,1,2,24]{3,2,1,0:T(2,128)(2,1)S(1)} %bitcast.101) | data formatting | bytes 393216
  110.5 3.8 %all-to-all-done.6 = bf16[16,16,1024]{2,1,0:T(8,128)(2,1)S(1)} async-done(((bf16[16,16,1024]{2,1,0:T(8,128)(2,1)}), bf16[16,16,1024]{2,1,0:T(8,128)(2,1)S(1)}, u32[]{:S(2)}, u32[]{:S(2)}) %all-to-all-start.6) | async-done | bytes 524320 | tf_op jit(solution)/shard_map/all_to_all | solution.py:44
  114.3 3.5 %all-to-all-start.5 = ((bf16[16,2,3072]{2,1,0:T(2,128)(2,1)}), bf16[16,2,3072]{2,1,0:T(2,128)(2,1)S(1)}, u32[]{:S(2)}, u32[]{:S(2)}) async-start(bf16[16,2,3072]{2,1,0:T(2,128)(2,1)} %reshape.315), calls=%async_computation.5 | async-start | bytes 393216 | tf_op jit(solution)/shard_map/all_to_all | solution.py:245
  118.0 7.0 %all-to-all-done.5 = bf16[16,2,3072]{2,1,0:T(2,128)(2,1)S(1)} async-done(((bf16[16,2,3072]{2,1,0:T(2,128)(2,1)}), bf16[16,2,3072]{2,1,0:T(2,128)(2,1)S(1)}, u32[]{:S(2)}, u32[]{:S(2)}) %all-to-all-start.5) | async-done | bytes 196640 | tf_op jit(solution)/shard_map/all_to_all | solution.py:245
  125.0 0.7 broadcast_in_dim.92
  125.7 3.7 %all-to-all-start.7 = ((bf16[16,16,512]{2,1,0:T(8,128)(2,1)}), bf16[16,16,512]{2,1,0:T(8,128)(2,1)S(1)}, u32[]{:S(2)}, u32[]{:S(2)}) async-start(bf16[16,16,512]{2,1,0:T(8,128)(2,1)} %broadcast_in_dim.92), calls=%async_computation.7 | async-start | bytes 524288 | tf_op jit(solution)/shard_map/all_to_all | solution.py:20
  129.4 0.2 copy.75
  129.7 1.5 reshape.316
  131.2 0.5 copy.78
  131.8 1.0 gather_fusion
  132.8 1.5 multiply_reduce_fusion
  134.3 2.4 %all-to-all-done.7 = bf16[16,16,512]{2,1,0:T(8,128)(2,1)S(1)} async-done(((bf16[16,16,512]{2,1,0:T(8,128)(2,1)}), bf16[16,16,512]{2,1,0:T(8,128)(2,1)S(1)}, u32[]{:S(2)}, u32[]{:S(2)}) %all-to-all-start.7) | async-done | bytes 262176 | tf_op jit(solution)/shard_map/all_to_all | solution.py:20
  136.7 0.2 fusion.13
  137.0 20.5 %all_to_all.60 = bf16[8,256,128]{2,1,0:T(8,128)(2,1)S(1)} all-to-all(bf16[8,256,128]{2,1,0:T(8,128)(2,1)S(1)} %broadcast_in_dim.93), channel_id=1, replica_groups=mesh['ep_0'=4,'ep_1'=4,'tp'=8] {'tp'}, dimensions={0} | all-to-all | bytes 1048576 | tf_op jit(solution)/shard_map/all_to_all | solution.py:20
  157.6 0.7 fusion.36
  (79 shorter events, 2.8 us)
Async XLA Ops:
  0.6 105.4 %copy-start = (bf16[2,128,2048]{2,1,0:T(8,128)(2,1)S(1)}, bf16[2,128,2048]{2,1,0:T(8,128)(2,1)}, u32[]{:S(2)}) copy-start(bf16[2,128,2048]{2,1,0:T(8,128)(2,1)} %param.45) | copy-start | bytes 3145732
  5.3 21.8 %all-to-all-start = ((bf16[16,16,512]{2,1,0:T(8,128)(2,1)}), bf16[16,16,512]{2,1,0:T(8,128)(2,1)S(1)}, u32[]{:S(2)}, u32[]{:S(2)}) async-start(bf16[16,16,512]{2,1,0:T(8,128)(2,1)} %pad_maximum_fusion.1), calls=%async_computation | async-start | bytes 524288 | tf_op jit(solution)/shard_map/all_to_all | solution.py:44
  18.8 6.8 %copy-start.14 = (f32[16]{0:T(128)S(1)}, f32[16]{0:T(128)}, u32[]{:S(2)}) copy-start(f32[16]{0:T(128)} %param.28) | copy-start | bytes 196
  18.8 8.2 %copy-start.12 = (s32[16]{0:T(128)S(1)}, s32[16]{0:T(128)}, u32[]{:S(2)}) copy-start(s32[16]{0:T(128)} %param.37) | copy-start | bytes 196
  18.8 16.1 %copy-start.10 = (f32[128]{0:T(128)S(1)}, f32[128]{0:T(128)}, u32[]{:S(2)}) copy-start(f32[128]{0:T(128)} %param.32) | copy-start | bytes 1540
  18.8 23.8 %copy-start.11 = (f32[128]{0:T(128)S(1)}, f32[128]{0:T(128)}, u32[]{:S(2)}) copy-start(f32[128]{0:T(128)} %param.33) | copy-start | bytes 1540
  18.9 24.7 %copy-start.3 = (f32[16,2,1024]{2,1,0:T(2,128)S(1)}, f32[16,2,1024]{2,1,0:T(2,128)}, u32[]{:S(2)}) copy-start(f32[16,2,1024]{2,1,0:T(2,128)} %param.36) | copy-start | bytes 393220
  27.9 14.3 %all-to-all-start.1 = ((f32[16,1,4352]{2,1,0:T(1,128)}), f32[16,1,4352]{2,1,0:T(1,128)S(1)}, u32[]{:S(2)}, u32[]{:S(2)}) async-start(f32[16,1,4352]{2,1,0:T(1,128)} %broadcast_in_dim.84), calls=%async_computation.1 | async-start | bytes 557056 | tf_op jit(solution)/shard_map/all_to_all | solution.py:20
  42.5 5.0 %copy-start.13 = (bf16[16,1,1024,128]{3,2,1,0:T(8,128)(2,1)S(1)}, bf16[16,1,1024,128]{3,2,1,0:T(8,128)(2,1)}, u32[]{:S(2)}) copy-start(bf16[16,1,1024,128]{3,2,1,0:T(8,128)(2,1)} %param.35) | copy-start | bytes 12582916
  43.3 5.0 %copy-start.8 = (bf16[16,128]{1,0:T(8,128)(2,1)}, bf16[16,128]{1,0:T(8,128)(2,1)S(1)}, u32[]{:S(2)}) copy-start(bf16[16,128]{1,0:T(8,128)(2,1)S(1)} %get-tuple-element.17) | copy-start | bytes 12292
  43.5 15.8 %copy-start.7 = (bf16[256,128]{1,0:T(8,128)(2,1)S(1)}, bf16[256,128]{1,0:T(8,128)(2,1)}, u32[]{:S(2)}) copy-start(bf16[256,128]{1,0:T(8,128)(2,1)} %param.38) | copy-start | bytes 196612
  47.6 30.5 %copy-start.1 = (bf16[256,128]{1,0:T(8,128)(2,1)S(1)}, bf16[256,128]{1,0:T(8,128)(2,1)}, u32[]{:S(2)}) copy-start(bf16[256,128]{1,0:T(8,128)(2,1)} %param.25) | copy-start | bytes 196612
  47.6 30.6 %copy-start.4 = (bf16[128,512]{1,0:T(8,128)(2,1)S(1)}, bf16[128,512]{1,0:T(8,128)(2,1)}, u32[]{:S(2)}) copy-start(bf16[128,512]{1,0:T(8,128)(2,1)} %param.47) | copy-start | bytes 393220
  47.6 30.8 %copy-start.5 = (bf16[128,512]{1,0:T(8,128)(2,1)S(1)}, bf16[128,512]{1,0:T(8,128)(2,1)}, u32[]{:S(2)}) copy-start(bf16[128,512]{1,0:T(8,128)(2,1)} %param.48) | copy-start | bytes 393220
  49.0 10.3 %all-to-all-start.2 = ((bf16[16,16,256]{2,1,0:T(8,128)(2,1)}), bf16[16,16,256]{2,1,0:T(8,128)(2,1)S(1)}, u32[]{:S(2)}, u32[]{:S(2)}) async-start(bf16[16,16,256]{2,1,0:T(8,128)(2,1)} %broadcast_in_dim.86), calls=%async_computation.2 | async-start | bytes 262144 | tf_op jit(solution)/shard_map/all_to_all | solution.py:20
  53.2 52.6 %copy-start.2 = (bf16[2,2048,128]{2,1,0:T(8,128)(2,1)S(1)}, bf16[2,2048,128]{2,1,0:T(8,128)(2,1)}, u32[]{:S(2)}) copy-start(bf16[2,2048,128]{2,1,0:T(8,128)(2,1)} %param.43) | copy-start | bytes 3145732
  60.3 17.6 %all-to-all-start.3 = ((bf16[8,256,128]{2,1,0:T(8,128)(2,1)}), bf16[8,256,128]{2,1,0:T(8,128)(2,1)S(1)}, u32[]{:S(2)}, u32[]{:S(2)}) async-start(bf16[8,256,128]{2,1,0:T(8,128)(2,1)} %broadcast_in_dim.87), calls=%async_computation.3 | async-start | bytes 1048576 | tf_op jit(solution)/shard_map/all_to_all | solution.py:20
  80.4 21.3 %all-to-all-start.4 = ((bf16[16,2,24,128]{3,2,1,0:T(8,128)(2,1)}), bf16[16,2,24,128]{3,2,1,0:T(8,128)(2,1)S(1)}, u32[]{:S(2)}, u32[]{:S(2)}) async-start(bf16[16,2,24,128]{3,2,1,0:T(8,128)(2,1)} %bitcast.13), calls=%async_computation.4 | async-start | bytes 393216 | tf_op jit(solution)/shard_map/all_to_all | solution.py:223
  101.7 12.5 %all-to-all-start.6 = ((bf16[16,16,1024]{2,1,0:T(8,128)(2,1)}), bf16[16,16,1024]{2,1,0:T(8,128)(2,1)S(1)}, u32[]{:S(2)}, u32[]{:S(2)}) async-start(bf16[16,16,1024]{2,1,0:T(8,128)(2,1)} %pad_maximum_fusion), calls=%async_computation.6 | async-start | bytes 1048576 | tf_op jit(solution)/shard_map/all_to_all | solution.py:44
  105.7 23.9 %copy-start.9 = (f32[256,2]{0,1:T(2,128)S(1)}, f32[256,2]{0,1:T(2,128)}, u32[]{:S(2)}) copy-start(f32[256,2]{0,1:T(2,128)} %param.42) | copy-start | bytes 6148
  108.5 28.2 %copy-start.6 = (bf16[512,128]{1,0:T(8,128)(2,1)S(1)}, bf16[512,128]{1,0:T(8,128)(2,1)}, u32[]{:S(2)}) copy-start(bf16[512,128]{1,0:T(8,128)(2,1)} %param.49) | copy-start | bytes 393220
  114.3 10.7 %all-to-all-start.5 = ((bf16[16,2,3072]{2,1,0:T(2,128)(2,1)}), bf16[16,2,3072]{2,1,0:T(2,128)(2,1)S(1)}, u32[]{:S(2)}, u32[]{:S(2)}) async-start(bf16[16,2,3072]{2,1,0:T(2,128)(2,1)} %reshape.315), calls=%async_computation.5 | async-start | bytes 393216 | tf_op jit(solution)/shard_map/all_to_all | solution.py:245
  125.7 11.0 %all-to-all-start.7 = ((bf16[16,16,512]{2,1,0:T(8,128)(2,1)}), bf16[16,16,512]{2,1,0:T(8,128)(2,1)S(1)}, u32[]{:S(2)}, u32[]{:S(2)}) async-start(bf16[16,16,512]{2,1,0:T(8,128)(2,1)} %broadcast_in_dim.92), calls=%async_computation.7 | async-start | bytes 524288 | tf_op jit(solution)/shard_map/all_to_all | solution.py:20
where the time goes:
time: 160 us; the launch traced here: 158 us
  starting transfers between devices  41.2 us (26%)
  blocking collectives  37.4 us (23%)
  waiting for transfers between devices  34.4 us (22%)
  local copies, waits for them, and re-layouts  19.7 us (12%)
  matrix products  13.1 us (8%)
  other arithmetic  11.2 us (7%)
    all_to_all x4, waiting for transfers between devices, from_everyone(): return lax.all_to_all(copies, axis, split_axis=0, concat_axis=0, tiled=True)  23.7 us
    all_to_all x4, starting transfers between devices, from_everyone(): return lax.all_to_all(copies, axis, split_axis=0, concat_axis=0, tiled=True)  22.2 us
    all_to_all x1, blocking collectives, from_everyone(): return lax.all_to_all(copies, axis, split_axis=0, concat_axis=0, tiled=True)  20.5 us
    psum x2, blocking collectives, by_axis(): shard = lax.psum(shard, axis)  16.9 us
    all_to_all x2, starting transfers between devices, summed_on_arrival(): lax.all_to_all(blocks, axis, split_axis=0, concat_axis=0, tiled=True)  12 us
    unnamed x36, local copies, waits for them, and re-layouts  9.33 us
    all_to_all x1, waiting for transfers between devices, on_device(): lax.all_to_all(expert_part[None].astype(jnp.bfloat16), EP, split_axis=3,...  6.97 us
    all_to_all x2, waiting for transfers between devices, summed_on_arrival(): lax.all_to_all(blocks, axis, split_axis=0, concat_axis=0, tiled=True)  3.76 us
  transfers between devices with their start and end apart: 8, of which 6 were waited for; matrix products, arithmetic and copies ran while one was open for 17% of the time, Pallas kernels for 0%

commit v1 on v0

v1 whole, which is shorter than its diff:
```python
import jax
import jax.numpy as jnp
from jax import lax
from jax.experimental import pallas as pl
from jax.experimental.pallas import tpu as pltpu
from jax.sharding import PartitionSpec as P

D = 2048
HEAD = 128
GROUP_EXPERTS = 4
CAPACITY = 24
EXPERTS = 32
SEQS = 256
EP = 16
TP = 8
OWN = SEQS // EP
EPS = 1e-06
FACTOR = HEAD**-0.5
F32 = jnp.float32
BF16 = jnp.bfloat16
MESH_ID = pl.DeviceIdType.MESH
NT = (((1,), (1,)), ((), ()))

EP_OFFSETS = sorted(
    [(dz, dx) for dz in range(4) for dx in range(4) if (dz, dx) != (0, 0)],
    key=lambda o: -(min(o[0], 4 - o[0]) + min(o[1], 4 - o[1])),
)
TP_OFFSETS = [4, 5, 3, 2, 6, 7, 1]


def mm(a, b):
    return jnp.dot(a, b, preferred_element_type=F32)


def iota(shape, dim):
    return lax.broadcasted_iota(jnp.int32, shape, dim)


def silu(v):
    return v * jax.nn.sigmoid(v)


def layer(
    hidden, attn_gain, forget_t, forget_bias, query_w, key_w, value_w, query_gain, key_gain,
    cache_k, cache_v, cache_g, lengths, output_w, ffn_gain, group, expert_t, weight_t,
    gate_w, up_w, down_w, mix_vector, dense_gate, dense_up, dense_down,
    mixed_out, keys_out, values_out,
    hid, again, fwt, fbias, wqkv, qgain, kgain, kcat, vbuf, graw, lens, wout, fgain,
    grp, ext, wtt, wgu, wdn, mixv, wdense, wdd,
    send1, recv1, gates, place, place_t, heads, part, psend, precv, mid,
    send4, xrows, send4d, recv4d, send5, ret, dhid, part2, psend2, precv2, final,
    load_sem, kv_sem, ep_send, ep_recv, tp_send, tp_recv, out_sem,
):
    e = lax.axis_index("ep")
    t = lax.axis_index("tp")
    z = lax.div(e, 4)
    x = lax.rem(e, 4)
    ep_peers = [
        (dz * 4 + dx, lax.rem(z + dz, 4) * 4 + lax.rem(x + dx, 4)) for dz, dx in EP_OFFSETS
    ]
    tp_peers = [(j, lax.rem(t + j, TP)) for j in TP_OFFSETS]
    own_cols = pl.ds(pl.multiple_of(e * HEAD, HEAD), HEAD)

    barrier = pltpu.get_barrier_semaphore()
    for _, peer in ep_peers:
        pl.semaphore_signal(barrier, inc=1, device_id={"ep": peer}, device_id_type=MESH_ID)
    for _, peer in tp_peers:
        pl.semaphore_signal(barrier, inc=1, device_id={"tp": peer}, device_id_type=MESH_ID)

    loads = {}

    def load(name, src, dst):
        copy = pltpu.make_async_copy(src, dst, load_sem.at[len(loads)])
        copy.start()
        loads[name] = copy

    load("hid", hidden, hid)
    load("again", attn_gain, again)
    load("fwt", forget_t.at[:, own_cols], fwt.at[pl.ds(0, 16)])
    load("wq", query_w, wqkv.at[:, pl.ds(0, 256)])
    load("wk", key_w, wqkv.at[:, pl.ds(256, 128)])
    load("wv", value_w, wqkv.at[:, pl.ds(384, 128)])
    load("grp", group, grp)
    load("ext", expert_t, ext)
    load("wtt", weight_t, wtt)
    load("graw", cache_g, graw)
    load("lens", lengths, lens)
    load("fbias", forget_bias, fbias)
    load("qgain", query_gain, qgain)
    load("kgain", key_gain, kgain)
    kv = []
    for b in range(OWN):
        copy = pltpu.make_async_copy(
            cache_k.at[b], kcat.at[:, pl.ds(b * HEAD, HEAD)], kv_sem.at[0, b]
        )
        copy.start()
        kv.append(copy)
    for b in range(OWN):
        copy = pltpu.make_async_copy(cache_v.at[b], vbuf.at[b], kv_sem.at[1, b])
        copy.start()
        kv.append(copy)
    load("wout", output_w, wout)
    load("fgain", ffn_gain, fgain)
    load("mixv", mix_vector, mixv)
    load("dg", dense_gate, wdense.at[:, pl.ds(0, 512)])
    load("du", dense_up, wdense.at[:, pl.ds(512, 512)])
    load("dd", dense_down, wdd)
    for i in range(2):
        load(f"g{i}", gate_w.at[i], wgu.at[:, pl.ds(i * 128, 128)])
        load(f"u{i}", up_w.at[i], wgu.at[:, pl.ds(256 + i * 128, 128)])
        load(f"d{i}", down_w.at[i], wdn.at[pl.ds(i * 128, 128)])

    def arrived(*names):
        for name in names:
            loads[name].wait()

    def to_ep(stage, src_of, dst_of):
        copies = []
        for j, peer in ep_peers:
            copy = pltpu.make_async_remote_copy(
                src_ref=src_of(peer),
                dst_ref=dst_of(j),
                send_sem=ep_send.at[stage, j],
                recv_sem=ep_recv.at[stage, j],
                device_id={"ep": peer},
                device_id_type=MESH_ID,
            )
            copy.start()
            copies.append(copy)
        return copies

    def to_tp(stage, src_of, dst_of):
        copies = []
        for j, peer in tp_peers:
            copy = pltpu.make_async_remote_copy(
                src_ref=src_of(peer),
                dst_ref=dst_of(j),
                send_sem=tp_send.at[stage, j],
                recv_sem=tp_recv.at[stage, j],
                device_id={"tp": peer},
                device_id_type=MESH_ID,
            )
            copy.start()
            copies.append(copy)
        return copies

    def landed(copies):
        for copy in copies:
            copy.wait_recv()

    fwt[pl.ds(16, 112), :] = jnp.zeros((112, HEAD), BF16)
    arrived("hid", "again", "fwt", "wq", "wk", "wv")
    stream = hid[...].astype(F32)
    normed = (stream * again[:, own_cols]).astype(BF16)
    projected = mm(normed, wqkv[...]).astype(BF16)
    send1[:, :, 0:512] = projected.reshape(EP, OWN, 512)
    stats = lax.dot_general(normed, fwt[...], NT, preferred_element_type=F32)
    lane = iota((SEQS, HEAD), 1)
    stats = jnp.where(lane == 16, jnp.sum(stream * stream, axis=1, keepdims=True), stats)
    high = stats.astype(BF16).astype(F32)
    low = stats - high
    both = jnp.where(lane < 64, high, pltpu.roll(low, 64, 1)).astype(BF16)
    send1[:, :, 512:640] = both.reshape(EP, OWN, HEAD)
    pl.semaphore_wait(barrier, EP + TP - 2)
    sent = to_ep(0, lambda peer: send1.at[peer], lambda j: recv1.at[j])
    first = sent

    arrived("grp", "ext", "wtt")
    chosen = [grp[...] * GROUP_EXPERTS + ext[pl.ds(k, 1), :] for k in range(2)]
    expert_row = iota((EXPERTS, SEQS), 0)
    hits = [jnp.where(expert_row == chosen[k], 1.0, 0.0) for k in range(2)]
    any_hit = hits[0] + hits[1]
    before = jnp.where(iota((SEQS, SEQS), 0) < iota((SEQS, SEQS), 1), 1.0, 0.0).astype(BF16)
    rank = mm(any_hit.astype(BF16), before)
    slot_of = rank + (expert_row * CAPACITY).astype(F32)
    slots = [
        jnp.sum(hits[k] * slot_of, axis=0, keepdims=True).astype(jnp.int32) for k in range(2)
    ]
    slot_row = iota((EXPERTS * CAPACITY, SEQS), 0)
    place[...] = jnp.where((slot_row == slots[0]) | (slot_row == slots[1]), 1.0, 0.0).astype(BF16)
    own_slot = iota((48, SEQS), 0) + e * 48
    slot_weight = jnp.sum(
        jnp.where(own_slot == slots[0], wtt[pl.ds(0, 1), :], 0.0)
        + jnp.where(own_slot == slots[1], wtt[pl.ds(1, 1), :], 0.0),
        axis=1,
        keepdims=True,
    )
    row8 = iota((8, SEQS), 0)
    slot_cols = jnp.where(row8 == 0, slots[0], slots[1]).astype(F32).T.astype(jnp.int32)
    slot_lane = iota((SEQS, EXPERTS * CAPACITY), 1)
    place_t[...] = jnp.where(
        (slot_lane == slot_cols[:, 0:1]) | (slot_lane == slot_cols[:, 1:2]), 1.0, 0.0
    ).astype(BF16)

    arrived("graw", "lens", "fbias", "qgain", "kgain")
    for b in range(OWN):
        for h in range(2):
            gates[pl.ds(h * OWN + b, 1), :] = graw[b, pl.ds(h, 1), :]
    seq_row = lax.rem(iota((2 * OWN, OWN), 0), OWN)
    len_col = jnp.sum(
        jnp.where(seq_row == iota((2 * OWN, OWN), 1), lens[...].astype(F32), 0.0),
        axis=1,
        keepdims=True,
    ).astype(jnp.int32)
    position = iota((2 * OWN, 1024), 1)
    gate_rows = gates[...]
    latest = jnp.sum(jnp.where(position == len_col - 1, gate_rows, 0.0), axis=1, keepdims=True)
    gates[...] = jnp.where(position < len_col, -gate_rows, -jnp.inf)
    lane16 = iota((1, 16), 1)
    bias = [
        jnp.sum(jnp.where(lane16 == 2 * t + h, fbias[...], 0.0), axis=1, keepdims=True)
        for h in range(2)
    ]
    for copy in kv:
        copy.wait()

    landed(first)
    sums = send1[e].astype(F32)
    for j in range(1, EP):
        sums = sums + recv1[j].astype(F32)
    stat = sums[:, 512:640]
    stat = stat + pltpu.roll(stat, 64, 1)
    lane = iota((OWN, HEAD), 1)

    def stat_at(index):
        return jnp.sum(jnp.where(lane == index, stat, 0.0), axis=1, keepdims=True)

    scale = lax.rsqrt(stat_at(16) / D + EPS)
    forget = []
    for h in range(2):
        logit = stat_at(2 * t + h) * scale + bias[h]
        forget.append(jnp.minimum(logit, 0.0) - jnp.log(1.0 + jnp.exp(-jnp.abs(logit))))

    def head_norm(rows, gain):
        mean = jnp.mean(rows * rows, axis=1, keepdims=True)
        return (rows * lax.rsqrt(mean + EPS) * gain).astype(BF16)

    queries = jnp.concatenate(
        [head_norm(sums[:, h * HEAD : (h + 1) * HEAD], qgain[...]) for h in range(2)], axis=0
    ).astype(F32)
    new_key = head_norm(sums[:, 256:384], kgain[...])
    new_value = (sums[:, 384:512] * scale).astype(BF16)
    keys_out[...] = new_key
    values_out[...] = new_value
    twice_key = jnp.concatenate([new_key, new_key], axis=0).astype(F32)
    twice_value = jnp.concatenate([new_value, new_value], axis=0).astype(F32)
    now = latest + jnp.concatenate(forget, axis=0)
    self_score = jnp.sum(queries * twice_key, axis=1, keepdims=True) * FACTOR

    q_row = lax.rem(iota((2 * OWN, HEAD), 0), OWN)
    spread = jnp.concatenate(
        [jnp.where(q_row == b, queries, 0.0).astype(BF16) for b in range(OWN)], axis=1
    )
    scores = lax.dot_general(spread, kcat[...], NT, preferred_element_type=F32)
    scores = scores * FACTOR + now + gates[...]
    ceiling = jnp.maximum(jnp.max(scores, axis=1, keepdims=True), self_score)
    weights = jnp.exp(scores - ceiling)
    self_weight = jnp.exp(self_score - ceiling)
    denominator = jnp.sum(weights, axis=1, keepdims=True) + self_weight
    p_row = lax.rem(iota((2 * OWN, 1024), 0), OWN)
    out = self_weight * twice_value
    for b in range(OWN):
        out = out + mm(jnp.where(p_row == b, weights, 0.0).astype(BF16), vbuf[b])
    out = out / denominator
    heads[e] = jnp.concatenate([out[0:OWN], out[OWN : 2 * OWN]], axis=1).astype(BF16)

    second = to_ep(1, lambda peer: heads.at[e], lambda j: heads.at[e])
    arrived("wout", "fgain", "mixv", "dg", "du", "dd", "g0", "g1", "u0", "u1", "d0", "d1")
    landed(second)
    attn = mm(heads[...].reshape(SEQS, 256), wout[...])
    own_rows = pl.ds(pl.multiple_of(t * 32, 32), 32)
    part[...] = attn
    psend[...] = attn.astype(BF16).reshape(TP, 32, HEAD)
    third = to_tp(0, lambda peer: psend.at[peer], lambda j: precv.at[j])
    landed(third)
    total = hid[own_rows, :].astype(F32) + part[own_rows, :]
    for j in range(1, TP):
        total = total + precv[j].astype(F32)
    mid[own_rows, :] = total.astype(BF16)
    fourth = to_tp(1, lambda peer: mid.at[own_rows], lambda j: mid.at[own_rows])
    landed(fourth)

    middle = mid[...]
    send4[:, 0:48, :] = mm(place[...], middle).astype(BF16).reshape(EP, 48, HEAD)
    send4[:, 48:64, :] = middle.reshape(EP, OWN, HEAD)
    rows = to_ep(2, lambda peer: send4.at[peer], lambda j: xrows.at[:, own_cols])
    normed_mid = (middle.astype(F32) * fgain[:, own_cols]).astype(BF16)
    send4d[...] = mm(normed_mid, wdense[...]).astype(BF16).reshape(EP, OWN, 1024)
    dense = to_ep(3, lambda peer: send4d.at[peer], lambda j: recv4d.at[j])
    xrows[:, own_cols] = send4[e]
    landed(rows)

    routed = xrows[0:48, :].astype(F32)
    slot_scale = lax.rsqrt(jnp.sum(routed * routed, axis=1, keepdims=True) / D + EPS)
    routed_in = (routed * fgain[...]).astype(BF16)
    both_pre = mm(routed_in, wgu[...])
    upper = iota((48, HEAD), 0) < CAPACITY
    gate_pre = jnp.where(upper, both_pre[:, 0:128], both_pre[:, 128:256]) * slot_scale
    up_pre = jnp.where(upper, both_pre[:, 256:384], both_pre[:, 384:512]) * slot_scale
    unit = silu(gate_pre) * up_pre
    units = jnp.concatenate(
        [jnp.where(upper, unit, 0.0), jnp.where(upper, 0.0, unit)], axis=1
    ).astype(BF16)
    send5[...] = (mm(units, wdn[...]) * slot_weight).astype(BF16)
    back = to_ep(
        4,
        lambda peer: send5.at[:, pl.ds(pl.multiple_of(peer * HEAD, HEAD), HEAD)],
        lambda j: ret.at[e],
    )
    ret[e] = send5[:, own_cols]

    own_mid = xrows[48:64, :].astype(F32)
    mid_scale = lax.rsqrt(jnp.sum(own_mid * own_mid, axis=1, keepdims=True) / D + EPS)
    own_normed = (own_mid * fgain[...]).astype(BF16).astype(F32)
    mix_dot = jnp.sum(own_normed * mixv[...].astype(F32), axis=1, keepdims=True)
    share = jax.nn.sigmoid(mid_scale * mix_dot)
    landed(dense)
    dsums = send4d[e].astype(F32)
    for j in range(1, EP):
        dsums = dsums + recv4d[j].astype(F32)
    dense_unit = silu(dsums[:, 0:512] * mid_scale) * (dsums[:, 512:1024] * mid_scale)
    dhid[e] = (dense_unit * share).astype(BF16)
    hidden_copies = to_ep(5, lambda peer: dhid.at[e], lambda j: dhid.at[e])

    landed(back)
    branch = mm(place_t[...], ret[...].reshape(EXPERTS * CAPACITY, HEAD))
    landed(hidden_copies)
    branch = branch + mm(dhid[...].reshape(SEQS, 512), wdd[...])
    part2[...] = branch
    psend2[...] = branch.astype(BF16).reshape(TP, 32, HEAD)
    fifth = to_tp(2, lambda peer: psend2.at[peer], lambda j: precv2.at[j])
    landed(fifth)
    total = mid[own_rows, :].astype(F32) + part2[own_rows, :]
    for j in range(1, TP):
        total = total + precv2[j].astype(F32)
    final[own_rows, :] = total.astype(BF16)
    sixth = to_tp(3, lambda peer: final.at[own_rows], lambda j: final.at[own_rows])
    landed(sixth)
    result = pltpu.make_async_copy(final, mixed_out, out_sem)
    result.start()
    for copies in (first, second, third, fourth, rows, dense, back, hidden_copies, fifth, sixth):
        for copy in copies:
            copy.wait_send()
    result.wait()


def on_device(
    hidden_in, attn_gain, forget_weight, forget_bias, query_weight, key_weight, value_weight,
    query_gain, key_gain, cache_keys, cache_values, cache_gates, lengths, output_weight,
    ffn_gain, route_group, route_expert, route_weight, expert_gate, expert_up, expert_down,
    mix_vector, dense_gate, dense_up, dense_down,
):
    vmem = pltpu.VMEM
    anywhere = pl.BlockSpec(memory_space=pl.ANY)
    scratch = [
        vmem((SEQS, HEAD), BF16),
        vmem((1, D), F32),
        vmem((HEAD, HEAD), BF16),
        vmem((1, 16), F32),
        vmem((HEAD, 512), BF16),
        vmem((1, HEAD), F32),
        vmem((1, HEAD), F32),
        vmem((1024, OWN * HEAD), BF16),
        vmem((OWN, 1024, HEAD), BF16),
        vmem((OWN, 2, 1024), F32),
        vmem((1, OWN), jnp.int32),
        vmem((256, HEAD), BF16),
        vmem((1, D), F32),
        vmem((1, SEQS), jnp.int32),
        vmem((2, SEQS), jnp.int32),
        vmem((2, SEQS), F32),
        vmem((D, 512), BF16),
        vmem((256, D), BF16),
        vmem((1, D), BF16),
        vmem((HEAD, 1024), BF16),
        vmem((512, HEAD), BF16),
        vmem((EP, OWN, 640), BF16),
        vmem((EP, OWN, 640), BF16),
        vmem((2 * OWN, 1024), F32),
        vmem((EXPERTS * CAPACITY, SEQS), BF16),
        vmem((SEQS, EXPERTS * CAPACITY), BF16),
        vmem((EP, OWN, 256), BF16),
        vmem((SEQS, HEAD), F32),
        vmem((TP, 32, HEAD), BF16),
        vmem((TP, 32, HEAD), BF16),
        vmem((SEQS, HEAD), BF16),
        vmem((EP, 64, HEAD), BF16),
        vmem((64, D), BF16),
        vmem((EP, OWN, 1024), BF16),
        vmem((EP, OWN, 1024), BF16),
        vmem((48, D), BF16),
        vmem((EP, 48, HEAD), BF16),
        vmem((EP, OWN, 512), BF16),
        vmem((SEQS, HEAD), F32),
        vmem((TP, 32, HEAD), BF16),
        vmem((TP, 32, HEAD), BF16),
        vmem((SEQS, HEAD), BF16),
        pltpu.SemaphoreType.DMA((26,)),
        pltpu.SemaphoreType.DMA((2, OWN)),
        pltpu.SemaphoreType.DMA((6, EP)),
        pltpu.SemaphoreType.DMA((6, EP)),
        pltpu.SemaphoreType.DMA((4, TP)),
        pltpu.SemaphoreType.DMA((4, TP)),
        pltpu.SemaphoreType.DMA,
    ]
    call = pl.pallas_call(
        layer,
        out_shape=(
            jax.ShapeDtypeStruct((SEQS, HEAD), BF16),
            jax.ShapeDtypeStruct((OWN, HEAD), BF16),
            jax.ShapeDtypeStruct((OWN, HEAD), BF16),
        ),
        in_specs=[anywhere] * 25,
        out_specs=(
            anywhere,
            pl.BlockSpec(memory_space=pltpu.VMEM),
            pl.BlockSpec(memory_space=pltpu.VMEM),
        ),
        scratch_shapes=scratch,
        compiler_params=pltpu.CompilerParams(
            collective_id=0, has_side_effects=True, vmem_limit_bytes=60 * 1024 * 1024
        ),
    )
    return call(
        hidden_in,
        attn_gain.reshape(1, D),
        forget_weight.T,
        forget_bias.reshape(1, 16),
        query_weight,
        key_weight,
        value_weight,
        query_gain.reshape(1, HEAD),
        key_gain.reshape(1, HEAD),
        cache_keys.reshape(OWN, 1024, HEAD),
        cache_values.reshape(OWN, 1024, HEAD),
        cache_gates,
        lengths.reshape(1, OWN),
        output_weight,
        ffn_gain.reshape(1, D),
        route_group.reshape(1, SEQS),
        route_expert.T,
        route_weight.T,
        expert_gate,
        expert_up,
        expert_down,
        mix_vector.reshape(1, D),
        dense_gate,
        dense_up,
        dense_down,
    )


def solution(mesh):
    placed = (
        P(None, "ep"), P(), P(), P(), P("ep", "tp"), P("ep", "tp"), P("ep", "tp"), P(), P(),
        P("ep", "tp", None, None), P("ep", "tp", None, None), P("ep", "tp", None), P("ep"),
        P("tp", "ep"), P(), P(), P(), P(), P("ep", None, "tp"), P("ep", None, "tp"),
        P("ep", "tp", None), P(), P("ep", "tp"), P("ep", "tp"), P("tp", "ep"),
    )
    return jax.shard_map(
        on_device,
        mesh=mesh,
        in_specs=placed,
        out_specs=(P(None, "ep"), P("ep", "tp"), P("ep", "tp")),
        check_vma=False,
    )
```

time: 160 us -> 63.5 us (0.40)
  Pallas kernels: 0 us -> 57.3 us
  starting transfers between devices: 41.2 us -> 0 us
  blocking collectives: 37.4 us -> 0 us
  waiting for transfers between devices: 34.4 us -> 0 us
  local copies, waits for them, and re-layouts: 19.7 us -> 5.31 us
  matrix products: 13.1 us -> 0 us
  other arithmetic: 11.2 us -> 0 us
    pallas_call x0 -> x1, Pallas kernels: none -> 57.3 us  [on_device(): call(hidden_in, attn_gain.reshape(1, D), forget_weight.T, forget_bias.res...]
    all_to_all x8 -> x0, starting transfers between devices: 41.2 us -> none  [the longest x4 22.2 us: from_everyone(): return lax.all_to_all(copies, axis, split_axis=0, concat_axis=0, tiled=True)]
    all_to_all x8 -> x0, waiting for transfers between devices: 34.4 us -> none  [the longest x4 23.7 us: from_everyone(): return lax.all_to_all(copies, axis, split_axis=0, concat_axis=0, tiled=True)]
    all_to_all x1 -> x0, blocking collectives: 20.5 us -> none  [from_everyone(): return lax.all_to_all(copies, axis, split_axis=0, concat_axis=0, tiled=True)]
    psum x2 -> x0, blocking collectives: 16.9 us -> none  [by_axis(): shard = lax.psum(shard, axis)]
    dot_general x15 -> x0, matrix products: 13.1 us -> none  [the longest x1 3.72 us: on_device(): jnp.einsum('skgd,skcd->skgc', grouped, cache_keys, preferred_element_type...]
    unnamed x36 -> x3, local copies, waits for them, and re-layouts: 9.33 us -> 4.02 us
    reduce_sum x13 -> x0, other arithmetic: 3.62 us -> none  [the longest x1 1.45 us: on_device(): routed = jnp.sum(picked * route_weight[:, :, None], axis=1)]
  transfers between devices with their start and end apart: 8 -> 0, of which waited for: 6 -> 0; matrix products, arithmetic and copies ran while one was open for 17% -> 0% of each run, Pallas kernels for 0% -> 0%
where the time goes in v1:
time: 63.5 us; the launch traced here: 63.3 us
  Pallas kernels  57.3 us (90%)
  local copies, waits for them, and re-layouts  5.31 us (8%)
  between operations  0.64 us (1%)
    pallas_call x1, Pallas kernels, on_device(): call(hidden_in, attn_gain.reshape(1, D), forget_weight.T, forget_bias.res...  57.3 us
    unnamed x3, local copies, waits for them, and re-layouts  4.02 us
    reshape x1, local copies, waits for them, and re-layouts, on_device(): mix_vector.reshape(1, D)  1.29 us

profile of v1, /device:TPU:1, one launch (start us, length us, event | category | flops | bytes accessed | tf_op | source)
XLA Modules:
  0.0 63.3 jit_solution(602940421556579257)
XLA Ops:
  0.6 1.3 %reshape.45.mix_vector = bf16[1,2048]{1,0:T(2,128)(2,1)} reshape(bf16[2048]{0:T(1024)(128)(2,1)} %param.46) | data formatting | bytes 8192 | tf_op jit(solution)/shard_map/reshape | solution.py:446
  1.9 57.3 %shard_map.256 = (bf16[256,128]{1,0:T(8,128)(2,1)}, bf16[16,128]{1,0:T(8,128)(2,1)}, bf16[16,128]{1,0:T(8,128)(2,1)}) custom-call(bf16[256,128]{1,0:T(8,128)(2,1)} %hidden.1, f32[1,2048]{1,0:T(1,128)} %bitcast.15, bf16[16,2048]{1,0:T(8,128)(2,1)} %bitcast.14, f32[1,16]{1,0:T(1,128)} %bitcast.20, bf16[128,256]{1,0:T(8,128)(2,1)} %query_w.1, ...), custom_call_target="tpu_custom_call" | custom-call | tf_op jit(solution)/shard_map/pallas_call | solution.py:424
  59.2 1.5 %copy.31 = bf16[256,128]{1,0:T(8,128)(2,1)} copy(bf16[256,128]{1,0:T(8,128)(2,1)} %get-tuple-element.6) | data formatting | bytes 131072
  60.7 1.3 %copy.32 = bf16[16,128]{1,0:T(8,128)(2,1)} copy(bf16[16,128]{1,0:T(8,128)(2,1)} %get-tuple-element.7) | data formatting | bytes 8192
  62.0 1.3 %copy.33 = bf16[16,128]{1,0:T(8,128)(2,1)} copy(bf16[16,128]{1,0:T(8,128)(2,1)} %get-tuple-element.8) | data formatting | bytes 8192

commit v2 on v1

--- a/solution.py
+++ b/solution.py
@@ -14,6 +14,8 @@
 EP = 16
 TP = 8
 OWN = SEQS // EP
+CHUNKS = 2
+WIDE = 512 // CHUNKS
 EPS = 1e-06
 FACTOR = HEAD**-0.5
 F32 = jnp.float32
@@ -38,6 +40,19 @@
 
 def silu(v):
     return v * jax.nn.sigmoid(v)
+
+
+def put_out(mixed, keys, values, mixed_out, keys_out, values_out, sems):
+    copies = [
+        pltpu.make_async_copy(src, dst, sems.at[i])
+        for i, (src, dst) in enumerate(
+            ((mixed, mixed_out), (keys, keys_out), (values, values_out))
+        )
+    ]
+    for copy in copies:
+        copy.start()
+    for copy in copies:
+        copy.wait()
 
 
 def layer(
@@ -49,7 +64,7 @@
     grp, ext, wtt, wgu, wdn, mixv, wdense, wdd,
     send1, recv1, gates, place, place_t, heads, part, psend, precv, mid,
     send4, xrows, send4d, recv4d, send5, ret, dhid, part2, psend2, precv2, final,
-    load_sem, kv_sem, ep_send, ep_recv, tp_send, tp_recv, out_sem,
+    load_sem, kv_sem, ep_send, ep_recv, tp_send, tp_recv,
 ):
     e = lax.axis_index("ep")
     t = lax.axis_index("tp")
@@ -102,8 +117,10 @@
     load("wout", output_w, wout)
     load("fgain", ffn_gain, fgain)
     load("mixv", mix_vector, mixv)
-    load("dg", dense_gate, wdense.at[:, pl.ds(0, 512)])
-    load("du", dense_up, wdense.at[:, pl.ds(512, 512)])
+    for c in range(CHUNKS):
+        cols = pl.ds(c * WIDE, WIDE)
+        load(f"dg{c}", dense_gate.at[:, cols], wdense.at[:, pl.ds(2 * c * WIDE, WIDE)])
+        load(f"du{c}", dense_up.at[:, cols], wdense.at[:, pl.ds((2 * c + 1) * WIDE, WIDE)])
     load("dd", dense_down, wdd)
     for i in range(2):
         load(f"g{i}", gate_w.at[i], wgu.at[:, pl.ds(i * 128, 128)])
@@ -265,7 +282,8 @@
     heads[e] = jnp.concatenate([out[0:OWN], out[OWN : 2 * OWN]], axis=1).astype(BF16)
 
     second = to_ep(1, lambda peer: heads.at[e], lambda j: heads.at[e])
-    arrived("wout", "fgain", "mixv", "dg", "du", "dd", "g0", "g1", "u0", "u1", "d0", "d1")
+    arrived("wout", "fgain", "mixv", "dd", "g0", "g1", "u0", "u1", "d0", "d1")
+    arrived(*[f"dg{c}" for c in range(CHUNKS)], *[f"du{c}" for c in range(CHUNKS)])
     landed(second)
     attn = mm(heads[...].reshape(SEQS, 256), wout[...])
     own_rows = pl.ds(pl.multiple_of(t * 32, 32), 32)
@@ -285,8 +303,13 @@
     send4[:, 48:64, :] = middle.reshape(EP, OWN, HEAD)
     rows = to_ep(2, lambda peer: send4.at[peer], lambda j: xrows.at[:, own_cols])
     normed_mid = (middle.astype(F32) * fgain[:, own_cols]).astype(BF16)
-    send4d[...] = mm(normed_mid, wdense[...]).astype(BF16).reshape(EP, OWN, 1024)
-    dense = to_ep(3, lambda peer: send4d.at[peer], lambda j: recv4d.at[j])
+    dense = []
+    for c in range(CHUNKS):
+        dense_part = mm(normed_mid, wdense[:, 2 * c * WIDE : 2 * (c + 1) * WIDE])
+        send4d[c] = dense_part.astype(BF16).reshape(EP, OWN, 2 * WIDE)
+        dense.append(
+            to_ep(5 + c, lambda peer: send4d.at[c, peer], lambda j: recv4d.at[c, j])
+        )
     xrows[:, own_cols] = send4[e]
     landed(rows)
 
@@ -303,7 +326,7 @@
     ).astype(BF16)
     send5[...] = (mm(units, wdn[...]) * slot_weight).astype(BF16)
     back = to_ep(
-        4,
+        3,
         lambda peer: send5.at[:, pl.ds(pl.multiple_of(peer * HEAD, HEAD), HEAD)],
         lambda j: ret.at[e],
     )
@@ -312,20 +335,30 @@
     own_mid = xrows[48:64, :].astype(F32)
     mid_scale = lax.rsqrt(jnp.sum(own_mid * own_mid, axis=1, keepdims=True) / D + EPS)
     own_normed = (own_mid * fgain[...]).astype(BF16).astype(F32)
-    mix_dot = jnp.sum(own_normed * mixv[...].astype(F32), axis=1, keepdims=True)
+    mix_rows = mixv[...].astype(F32)
+    mix_dot = sum(
+        own_normed[:, s * HEAD : (s + 1) * HEAD] * mix_rows[s : s + 1] for s in range(EP)
+    ).sum(axis=1, keepdims=True)
     share = jax.nn.sigmoid(mid_scale * mix_dot)
-    landed(dense)
-    dsums = send4d[e].astype(F32)
-    for j in range(1, EP):
-        dsums = dsums + recv4d[j].astype(F32)
-    dense_unit = silu(dsums[:, 0:512] * mid_scale) * (dsums[:, 512:1024] * mid_scale)
-    dhid[e] = (dense_unit * share).astype(BF16)
-    hidden_copies = to_ep(5, lambda peer: dhid.at[e], lambda j: dhid.at[e])
+    hidden_copies = []
+    for c in range(CHUNKS):
+        landed(dense[c])
+        dsums = send4d[c, e].astype(F32)
+        for j in range(1, EP):
+            dsums = dsums + recv4d[c, j].astype(F32)
+        dense_unit = silu(dsums[:, :WIDE] * mid_scale) * (dsums[:, WIDE:] * mid_scale)
+        dhid[c, e] = (dense_unit * share).astype(BF16)
+        hidden_copies.append(
+            to_ep(5 + CHUNKS + c, lambda peer: dhid.at[c, e], lambda j: dhid.at[c, e])
+        )
 
     landed(back)
     branch = mm(place_t[...], ret[...].reshape(EXPERTS * CAPACITY, HEAD))
-    landed(hidden_copies)
-    branch = branch + mm(dhid[...].reshape(SEQS, 512), wdd[...])
+    for c in range(CHUNKS):
+        landed(hidden_copies[c])
+        branch = branch + mm(
+            dhid[c].reshape(SEQS, WIDE), wdd[c * WIDE : (c + 1) * WIDE, :]
+        )
     part2[...] = branch
     psend2[...] = branch.astype(BF16).reshape(TP, 32, HEAD)
     fifth = to_tp(2, lambda peer: psend2.at[peer], lambda j: precv2.at[j])
@@ -336,12 +369,11 @@
     final[own_rows, :] = total.astype(BF16)
     sixth = to_tp(3, lambda peer: final.at[own_rows], lambda j: final.at[own_rows])
     landed(sixth)
-    result = pltpu.make_async_copy(final, mixed_out, out_sem)
-    result.start()
-    for copies in (first, second, third, fourth, rows, dense, back, hidden_copies, fifth, sixth):
+    mixed_out[...] = final[...]
+    groups = [first, second, third, fourth, rows, back, fifth, sixth]
+    for copies in groups + dense + hidden_copies:
         for copy in copies:
             copy.wait_send()
-    result.wait()
 
 
 def on_device(
@@ -351,7 +383,7 @@
     mix_vector, dense_gate, dense_up, dense_down,
 ):
     vmem = pltpu.VMEM
-    anywhere = pl.BlockSpec(memory_space=pl.ANY)
+    anywhere = pl.BlockSpec(memory_space=pltpu.HBM)
     scratch = [
         vmem((SEQS, HEAD), BF16),
         vmem((1, D), F32),
@@ -371,7 +403,7 @@
         vmem((2, SEQS), F32),
         vmem((D, 512), BF16),
         vmem((256, D), BF16),
-        vmem((1, D), BF16),
+        vmem((16, HEAD), BF16),
         vmem((HEAD, 1024), BF16),
         vmem((512, HEAD), BF16),
         vmem((EP, OWN, 640), BF16),
@@ -386,42 +418,37 @@
         vmem((SEQS, HEAD), BF16),
         vmem((EP, 64, HEAD), BF16),
         vmem((64, D), BF16),
-        vmem((EP, OWN, 1024), BF16),
-        vmem((EP, OWN, 1024), BF16),
+        vmem((CHUNKS, EP, OWN, 2 * WIDE), BF16),
+        vmem((CHUNKS, EP, OWN, 2 * WIDE), BF16),
         vmem((48, D), BF16),
         vmem((EP, 48, HEAD), BF16),
-        vmem((EP, OWN, 512), BF16),
+        vmem((CHUNKS, EP, OWN, WIDE), BF16),
         vmem((SEQS, HEAD), F32),
         vmem((TP, 32, HEAD), BF16),
         vmem((TP, 32, HEAD), BF16),
         vmem((SEQS, HEAD), BF16),
-        pltpu.SemaphoreType.DMA((26,)),
+        pltpu.SemaphoreType.DMA((24 + 2 * CHUNKS,)),
         pltpu.SemaphoreType.DMA((2, OWN)),
-        pltpu.SemaphoreType.DMA((6, EP)),
-        pltpu.SemaphoreType.DMA((6, EP)),
+        pltpu.SemaphoreType.DMA((5 + 2 * CHUNKS, EP)),
+        pltpu.SemaphoreType.DMA((5 + 2 * CHUNKS, EP)),
         pltpu.SemaphoreType.DMA((4, TP)),
         pltpu.SemaphoreType.DMA((4, TP)),
-        pltpu.SemaphoreType.DMA,
     ]
     call = pl.pallas_call(
         layer,
         out_shape=(
-            jax.ShapeDtypeStruct((SEQS, HEAD), BF16),
-            jax.ShapeDtypeStruct((OWN, HEAD), BF16),
-            jax.ShapeDtypeStruct((OWN, HEAD), BF16),
+            vmem((SEQS, HEAD), BF16),
+            vmem((OWN, HEAD), BF16),
+            vmem((OWN, HEAD), BF16),
         ),
         in_specs=[anywhere] * 25,
-        out_specs=(
-            anywhere,
-            pl.BlockSpec(memory_space=pltpu.VMEM),
-            pl.BlockSpec(memory_space=pltpu.VMEM),
-        ),
+        out_specs=(pl.BlockSpec(memory_space=pltpu.VMEM),) * 3,
         scratch_shapes=scratch,
         compiler_params=pltpu.CompilerParams(
             collective_id=0, has_side_effects=True, vmem_limit_bytes=60 * 1024 * 1024
         ),
     )
-    return call(
+    results = call(
         hidden_in,
         attn_gain.reshape(1, D),
         forget_weight.T,
@@ -443,11 +470,19 @@
         expert_gate,
         expert_up,
         expert_down,
-        mix_vector.reshape(1, D),
+        mix_vector.reshape(16, HEAD),
         dense_gate,
         dense_up,
         dense_down,
     )
+    return pl.pallas_call(
+        put_out,
+        out_shape=[jax.ShapeDtypeStruct(r.shape, r.dtype) for r in results],
+        in_specs=[pl.BlockSpec(memory_space=pltpu.VMEM)] * 3,
+        out_specs=[anywhere] * 3,
+        scratch_shapes=[pltpu.SemaphoreType.DMA((3,))],
+        compiler_params=pltpu.CompilerParams(vmem_limit_bytes=1024 * 1024),
+    )(*results)
 
 
 def solution(mesh):

time: 63.5 us -> 58.6 us (0.923)
  local copies, waits for them, and re-layouts: 5.31 us -> 0 us
    unnamed x3 -> x0, local copies, waits for them, and re-layouts: 4.02 us -> none
    reshape x1 -> x0, local copies, waits for them, and re-layouts: 1.29 us -> none  [on_device(): mix_vector.reshape(1, D)]
    pallas_call x0 -> x1, Pallas kernels: none -> 0.66 us  [on_device(): pl.pallas_call(put_out, out_shape=[jax.ShapeDtypeStruct(r.shape, r.dtype)...]
where the time goes in v2:
time: 58.6 us; the launch traced here: 58.5 us
  Pallas kernels  57.8 us (99%)
  between operations  0.65 us (1%)
    pallas_call x1, Pallas kernels, on_device(): call(hidden_in, attn_gain.reshape(1, D), forget_weight.T, forget_bias.res...  57.1 us

profile of v2, /device:TPU:1, one launch (start us, length us, event | category | flops | bytes accessed | tf_op | source)
XLA Modules:
  0.0 58.5 jit_solution(12079903152843417242)
XLA Ops:
  0.6 57.1 %shard_map.256 = (bf16[256,128]{1,0:T(8,128)(2,1)S(1)}, bf16[16,128]{1,0:T(8,128)(2,1)S(1)}, bf16[16,128]{1,0:T(8,128)(2,1)S(1)}) custom-call(bf16[256,128]{1,0:T(8,128)(2,1)} %hidden.1, f32[1,2048]{1,0:T(1,128)} %bitcast.16, bf16[16,2048]{1,0:T(8,128)(2,1)} %bitcast.15, f32[1,16]{1,0:T(1,128)} %bitcast.22, bf16[128,256]{1,0:T(8,128)(2,1)} %query_w.1, ...), custom_call_target="tpu_custom_call" | custom-call | tf_op jit(solution)/shard_map/pallas_call | solution.py:451
  57.8 0.7 %shard_map.257 = (bf16[256,128]{1,0:T(8,128)(2,1)}, bf16[16,128]{1,0:T(8,128)(2,1)}, bf16[16,128]{1,0:T(8,128)(2,1)}) custom-call(bf16[256,128]{1,0:T(8,128)(2,1)S(1)} %get-tuple-element.6.mixed, bf16[16,128]{1,0:T(8,128)(2,1)S(1)} %get-tuple-element.7.keys, bf16[16,128]{1,0:T(8,128)(2,1)S(1)} %get-tuple-element.8.values), custom_call_target="tpu_custom_call" | custom-call | tf_op jit(solution)/shard_map/pallas_call | solution.py:478

commit v3 on v2

--- a/solution.py
+++ b/solution.py
@@ -12,7 +12,6 @@
 EXPERTS = 32
 SEQS = 256
 EP = 16
-TP = 8
 OWN = SEQS // EP
 CHUNKS = 2
 WIDE = 512 // CHUNKS
@@ -27,7 +26,6 @@
     [(dz, dx) for dz in range(4) for dx in range(4) if (dz, dx) != (0, 0)],
     key=lambda o: -(min(o[0], 4 - o[0]) + min(o[1], 4 - o[1])),
 )
-TP_OFFSETS = [4, 5, 3, 2, 6, 7, 1]
 
 
 def mm(a, b):
@@ -62,8 +60,8 @@
     mixed_out, keys_out, values_out,
     hid, again, fwt, fbias, wqkv, qgain, kgain, kcat, vbuf, graw, lens, wout, fgain,
     grp, ext, wtt, wgu, wdn, mixv, wdense, wdd,
-    send1, recv1, gates, place, place_t, heads, part, psend, precv, mid,
-    send4, xrows, send4d, recv4d, send5, ret, dhid, part2, psend2, precv2, final,
+    send1, recv1, gates, place, place_t, heads, halves, other, chips, mid,
+    send4, xrows, send4d, recv4d, send5, ret, dhid, halves2, other2, chips2, final,
     load_sem, kv_sem, ep_send, ep_recv, tp_send, tp_recv,
 ):
     e = lax.axis_index("ep")
@@ -73,13 +71,16 @@
     ep_peers = [
         (dz * 4 + dx, lax.rem(z + dz, 4) * 4 + lax.rem(x + dx, 4)) for dz, dx in EP_OFFSETS
     ]
-    tp_peers = [(j, lax.rem(t + j, TP)) for j in TP_OFFSETS]
+    y = lax.div(t, 2)
+    core = lax.rem(t, 2)
+    sibling = t + 1 - 2 * core
+    y_peers = [(j, lax.rem(y + j, 4) * 2 + core) for j in (2, 1, 3)]
     own_cols = pl.ds(pl.multiple_of(e * HEAD, HEAD), HEAD)
 
     barrier = pltpu.get_barrier_semaphore()
     for _, peer in ep_peers:
         pl.semaphore_signal(barrier, inc=1, device_id={"ep": peer}, device_id_type=MESH_ID)
-    for _, peer in tp_peers:
+    for peer in [peer for _, peer in y_peers] + [sibling]:
         pl.semaphore_signal(barrier, inc=1, device_id={"tp": peer}, device_id_type=MESH_ID)
 
     loads = {}
@@ -146,24 +147,41 @@
             copies.append(copy)
         return copies
 
-    def to_tp(stage, src_of, dst_of):
-        copies = []
-        for j, peer in tp_peers:
-            copy = pltpu.make_async_remote_copy(
-                src_ref=src_of(peer),
-                dst_ref=dst_of(j),
-                send_sem=tp_send.at[stage, j],
-                recv_sem=tp_recv.at[stage, j],
-                device_id={"tp": peer},
-                device_id_type=MESH_ID,
-            )
-            copy.start()
-            copies.append(copy)
-        return copies
+    def to_tp(peer, src, dst, index):
+        copy = pltpu.make_async_remote_copy(
+            src_ref=src,
+            dst_ref=dst,
+            send_sem=tp_send.at[index],
+            recv_sem=tp_recv.at[index],
+            device_id={"tp": peer},
+            device_id_type=MESH_ID,
+        )
+        copy.start()
+        return copy
 
     def landed(copies):
         for copy in copies:
             copy.wait_recv()
+
+    half = pl.ds(pl.multiple_of(core * 128, 128), 128)
+    tp_copies = []
+
+    def add_over_tp(stage, terms, base, halves, other, chips, dst):
+        halves[...] = terms.reshape(2, 128, HEAD)
+        pair = to_tp(sibling, halves.at[1 - core], other, 5 * stage)
+        pair.wait_recv()
+        chips[y] = (halves[core] + other[...]).astype(BF16)
+        along = [
+            to_tp(peer, chips.at[y], chips.at[y], 5 * stage + j) for j, peer in y_peers
+        ]
+        landed(along)
+        total = base[half, :].astype(F32)
+        for chip in range(4):
+            total = total + chips[chip].astype(F32)
+        dst[half, :] = total.astype(BF16)
+        last = to_tp(sibling, dst.at[half], dst.at[half], 5 * stage + 4)
+        last.wait_recv()
+        tp_copies.extend([pair, last, *along])
 
     fwt[pl.ds(16, 112), :] = jnp.zeros((112, HEAD), BF16)
     arrived("hid", "again", "fwt", "wq", "wk", "wv")
@@ -178,7 +196,7 @@
     low = stats - high
     both = jnp.where(lane < 64, high, pltpu.roll(low, 64, 1)).astype(BF16)
     send1[:, :, 512:640] = both.reshape(EP, OWN, HEAD)
-    pl.semaphore_wait(barrier, EP + TP - 2)
+    pl.semaphore_wait(barrier, EP - 1 + 4)
     sent = to_ep(0, lambda peer: send1.at[peer], lambda j: recv1.at[j])
     first = sent
 
@@ -193,8 +211,10 @@
     slots = [
         jnp.sum(hits[k] * slot_of, axis=0, keepdims=True).astype(jnp.int32) for k in range(2)
     ]
-    slot_row = iota((EXPERTS * CAPACITY, SEQS), 0)
-    place[...] = jnp.where((slot_row == slots[0]) | (slot_row == slots[1]), 1.0, 0.0).astype(BF16)
+    three = (EP, CAPACITY, SEQS)
+    slot_row = (2 * iota(three, 0) + core) * CAPACITY + iota(three, 1)
+    hit = (slot_row == slots[0][None]) | (slot_row == slots[1][None])
+    place[...] = jnp.where(hit, 1.0, 0.0).reshape(EP * CAPACITY, SEQS).astype(BF16)
     own_slot = iota((48, SEQS), 0) + e * 48
     slot_weight = jnp.sum(
         jnp.where(own_slot == slots[0], wtt[pl.ds(0, 1), :], 0.0)
@@ -286,22 +306,14 @@
     arrived(*[f"dg{c}" for c in range(CHUNKS)], *[f"du{c}" for c in range(CHUNKS)])
     landed(second)
     attn = mm(heads[...].reshape(SEQS, 256), wout[...])
-    own_rows = pl.ds(pl.multiple_of(t * 32, 32), 32)
-    part[...] = attn
-    psend[...] = attn.astype(BF16).reshape(TP, 32, HEAD)
-    third = to_tp(0, lambda peer: psend.at[peer], lambda j: precv.at[j])
-    landed(third)
-    total = hid[own_rows, :].astype(F32) + part[own_rows, :]
-    for j in range(1, TP):
-        total = total + precv[j].astype(F32)
-    mid[own_rows, :] = total.astype(BF16)
-    fourth = to_tp(1, lambda peer: mid.at[own_rows], lambda j: mid.at[own_rows])
-    landed(fourth)
+    add_over_tp(0, attn, hid, halves, other, chips, mid)
 
     middle = mid[...]
-    send4[:, 0:48, :] = mm(place[...], middle).astype(BF16).reshape(EP, 48, HEAD)
-    send4[:, 48:64, :] = middle.reshape(EP, OWN, HEAD)
-    rows = to_ep(2, lambda peer: send4.at[peer], lambda j: xrows.at[:, own_cols])
+    per_owner = middle.astype(F32).reshape(EP, OWN, HEAD)
+    own_part = jnp.where(core == 0, per_owner[:, 0:8], per_owner[:, 8:16])
+    picked = mm(place[...], middle).reshape(EP, CAPACITY, HEAD)
+    send4[...] = jnp.concatenate([picked, own_part], axis=1).astype(BF16)
+    rows = to_ep(2, lambda peer: send4.at[peer], lambda j: xrows.at[core, :, own_cols])
     normed_mid = (middle.astype(F32) * fgain[:, own_cols]).astype(BF16)
     dense = []
     for c in range(CHUNKS):
@@ -310,10 +322,14 @@
         dense.append(
             to_ep(5 + c, lambda peer: send4d.at[c, peer], lambda j: recv4d.at[c, j])
         )
-    xrows[:, own_cols] = send4[e]
+    xrows[core, :, own_cols] = send4[e]
     landed(rows)
-
-    routed = xrows[0:48, :].astype(F32)
+    shared = to_tp(sibling, xrows.at[core], xrows.at[core], 10)
+    shared.wait_recv()
+    tp_copies.append(shared)
+
+    arrived_rows = [xrows[k].astype(F32) for k in range(2)]
+    routed = jnp.concatenate([r[0:CAPACITY] for r in arrived_rows], axis=0)
     slot_scale = lax.rsqrt(jnp.sum(routed * routed, axis=1, keepdims=True) / D + EPS)
     routed_in = (routed * fgain[...]).astype(BF16)
     both_pre = mm(routed_in, wgu[...])
@@ -332,7 +348,7 @@
     )
     ret[e] = send5[:, own_cols]
 
-    own_mid = xrows[48:64, :].astype(F32)
+    own_mid = jnp.concatenate([r[CAPACITY:] for r in arrived_rows], axis=0)
     mid_scale = lax.rsqrt(jnp.sum(own_mid * own_mid, axis=1, keepdims=True) / D + EPS)
     own_normed = (own_mid * fgain[...]).astype(BF16).astype(F32)
     mix_rows = mixv[...].astype(F32)
@@ -359,18 +375,9 @@
         branch = branch + mm(
             dhid[c].reshape(SEQS, WIDE), wdd[c * WIDE : (c + 1) * WIDE, :]
         )
-    part2[...] = branch
-    psend2[...] = branch.astype(BF16).reshape(TP, 32, HEAD)
-    fifth = to_tp(2, lambda peer: psend2.at[peer], lambda j: precv2.at[j])
-    landed(fifth)
-    total = mid[own_rows, :].astype(F32) + part2[own_rows, :]
-    for j in range(1, TP):
-        total = total + precv2[j].astype(F32)
-    final[own_rows, :] = total.astype(BF16)
-    sixth = to_tp(3, lambda peer: final.at[own_rows], lambda j: final.at[own_rows])
-    landed(sixth)
+    add_over_tp(1, branch, mid, halves2, other2, chips2, final)
     mixed_out[...] = final[...]
-    groups = [first, second, third, fourth, rows, back, fifth, sixth]
+    groups = [first, second, rows, back, tp_copies]
     for copies in groups + dense + hidden_copies:
         for copy in copies:
             copy.wait_send()
@@ -409,30 +416,30 @@
         vmem((EP, OWN, 640), BF16),
         vmem((EP, OWN, 640), BF16),
         vmem((2 * OWN, 1024), F32),
-        vmem((EXPERTS * CAPACITY, SEQS), BF16),
+        vmem((EP * CAPACITY, SEQS), BF16),
         vmem((SEQS, EXPERTS * CAPACITY), BF16),
         vmem((EP, OWN, 256), BF16),
-        vmem((SEQS, HEAD), F32),
-        vmem((TP, 32, HEAD), BF16),
-        vmem((TP, 32, HEAD), BF16),
+        vmem((2, 128, HEAD), F32),
+        vmem((128, HEAD), F32),
+        vmem((4, 128, HEAD), BF16),
         vmem((SEQS, HEAD), BF16),
-        vmem((EP, 64, HEAD), BF16),
-        vmem((64, D), BF16),
+        vmem((EP, 32, HEAD), BF16),
+        vmem((2, 32, D), BF16),
         vmem((CHUNKS, EP, OWN, 2 * WIDE), BF16),
         vmem((CHUNKS, EP, OWN, 2 * WIDE), BF16),
         vmem((48, D), BF16),
         vmem((EP, 48, HEAD), BF16),
         vmem((CHUNKS, EP, OWN, WIDE), BF16),
-        vmem((SEQS, HEAD), F32),
-        vmem((TP, 32, HEAD), BF16),
-        vmem((TP, 32, HEAD), BF16),
+        vmem((2, 128, HEAD), F32),
+        vmem((128, HEAD), F32),
+        vmem((4, 128, HEAD), BF16),
         vmem((SEQS, HEAD), BF16),
         pltpu.SemaphoreType.DMA((24 + 2 * CHUNKS,)),
         pltpu.SemaphoreType.DMA((2, OWN)),
         pltpu.SemaphoreType.DMA((5 + 2 * CHUNKS, EP)),
         pltpu.SemaphoreType.DMA((5 + 2 * CHUNKS, EP)),
-        pltpu.SemaphoreType.DMA((4, TP)),
-        pltpu.SemaphoreType.DMA((4, TP)),
+        pltpu.SemaphoreType.DMA((11,)),
+        pltpu.SemaphoreType.DMA((11,)),
     ]
     call = pl.pallas_call(
         layer,

time: 58.6 us -> 52.9 us (0.903)
  Pallas kernels: 57.8 us -> 52.1 us
    pallas_call x1, Pallas kernels: 57.1 us -> 51.4 us  [on_device(): call(hidden_in, attn_gain.reshape(1, D), forget_weight.T, forget_bias.res...]
where the time goes in v3:
time: 52.9 us; the launch traced here: 52.8 us
  Pallas kernels  52.1 us (98%)
  between operations  0.65 us (1%)
    pallas_call x1, Pallas kernels, on_device(): call(hidden_in, attn_gain.reshape(1, D), forget_weight.T, forget_bias.res...  51.4 us

profile of v3, /device:TPU:1, one launch (start us, length us, event | category | flops | bytes accessed | tf_op | source)
XLA Modules:
  0.0 52.8 jit_solution(1180611527334396111)
XLA Ops:
  0.6 51.4 %shard_map.256 = (bf16[256,128]{1,0:T(8,128)(2,1)S(1)}, bf16[16,128]{1,0:T(8,128)(2,1)S(1)}, bf16[16,128]{1,0:T(8,128)(2,1)S(1)}) custom-call(bf16[256,128]{1,0:T(8,128)(2,1)} %hidden.1, f32[1,2048]{1,0:T(1,128)} %bitcast.16, bf16[16,2048]{1,0:T(8,128)(2,1)} %bitcast.15, f32[1,16]{1,0:T(1,128)} %bitcast.22, bf16[128,256]{1,0:T(8,128)(2,1)} %query_w.1, ...), custom_call_target="tpu_custom_call" | custom-call | tf_op jit(solution)/shard_map/pallas_call | solution.py:458
  52.1 0.7 %shard_map.257 = (bf16[256,128]{1,0:T(8,128)(2,1)}, bf16[16,128]{1,0:T(8,128)(2,1)}, bf16[16,128]{1,0:T(8,128)(2,1)}) custom-call(bf16[256,128]{1,0:T(8,128)(2,1)S(1)} %get-tuple-element.6.mixed, bf16[16,128]{1,0:T(8,128)(2,1)S(1)} %get-tuple-element.7.keys, bf16[16,128]{1,0:T(8,128)(2,1)S(1)} %get-tuple-element.8.values), custom_call_target="tpu_custom_call" | custom-call | tf_op jit(solution)/shard_map/pallas_call | solution.py:485

commit v4 on v3

--- a/solution.py
+++ b/solution.py
@@ -22,10 +22,7 @@
 MESH_ID = pl.DeviceIdType.MESH
 NT = (((1,), (1,)), ((), ()))
 
-EP_OFFSETS = sorted(
-    [(dz, dx) for dz in range(4) for dx in range(4) if (dz, dx) != (0, 0)],
-    key=lambda o: -(min(o[0], 4 - o[0]) + min(o[1], 4 - o[1])),
-)
+EP_OFFSETS = [(2, 2), (2, 1), (1, 2), (2, 3), (3, 2), (2, 0), (0, 2), (1, 1), (3, 3), (1, 3), (3, 1), (0, 1), (3, 0), (0, 3), (1, 0)]
 
 
 def mm(a, b):

time: 52.9 us -> 52.5 us (level)
  no operation moved by 1% of the time
where the time goes in v4:
time: 52.5 us; the launch traced here: 52.4 us
  Pallas kernels  51.7 us (98%)
  between operations  0.65 us (1%)
    pallas_call x1, Pallas kernels, on_device(): call(hidden_in, attn_gain.reshape(1, D), forget_weight.T, forget_bias.res...  51.1 us

profile of v4, /device:TPU:1, one launch (start us, length us, event | category | flops | bytes accessed | tf_op | source)
XLA Modules:
  0.0 52.4 jit_solution(16294892982193933955)
XLA Ops:
  0.6 51.1 %shard_map.256 = (bf16[256,128]{1,0:T(8,128)(2,1)S(1)}, bf16[16,128]{1,0:T(8,128)(2,1)S(1)}, bf16[16,128]{1,0:T(8,128)(2,1)S(1)}) custom-call(bf16[256,128]{1,0:T(8,128)(2,1)} %hidden.1, f32[1,2048]{1,0:T(1,128)} %bitcast.16, bf16[16,2048]{1,0:T(8,128)(2,1)} %bitcast.15, f32[1,16]{1,0:T(1,128)} %bitcast.22, bf16[128,256]{1,0:T(8,128)(2,1)} %query_w.1, ...), custom_call_target="tpu_custom_call" | custom-call | tf_op jit(solution)/shard_map/pallas_call | solution.py:455
  51.7 0.7 %shard_map.257 = (bf16[256,128]{1,0:T(8,128)(2,1)}, bf16[16,128]{1,0:T(8,128)(2,1)}, bf16[16,128]{1,0:T(8,128)(2,1)}) custom-call(bf16[256,128]{1,0:T(8,128)(2,1)S(1)} %get-tuple-element.6.mixed, bf16[16,128]{1,0:T(8,128)(2,1)S(1)} %get-tuple-element.7.keys, bf16[16,128]{1,0:T(8,128)(2,1)S(1)} %get-tuple-element.8.values), custom_call_target="tpu_custom_call" | custom-call | tf_op jit(solution)/shard_map/pallas_call | solution.py:482
